TPU v7x, 32 devices: a whole 2x2x4 slice. The times are simulated.
32 devices in a mesh: sp: 8 (over z, x), tp: 4 (over y, core).
Axes of the slice: x: 2, y: 2, z: 4, core: 2. Of those that a mesh axis runs over, the one named last changes fastest.
Arguments:
- query_matrix: bfloat16 [2048, 1024], P('sp', 'tp'), may hold values from -6 to 6
- key_matrix: bfloat16 [2048, 1024], P('sp', 'tp'), may hold values from -6 to 6
- value_matrix: bfloat16 [2048, 2048], P('sp', 'tp'), may hold values from -6 to 6
- output_gate_rows: bfloat16 [2048, 2048], P('sp', 'tp'), may hold values from -6 to 6
- decay_preactivation: bfloat16 [2048, 1024], P('sp', 'tp'), may hold values from -5 to 5
- channel_decay_bias: float32 [1024], P('tp'), may hold values from 0 to 10
- extra_log_decay: float32 [2048, 16], P('sp', 'tp'), may hold values from -0.7 to 0
- head_norm_gain: float32 [128], replicated, may hold values from 0.1 to 1.9
- output_projection: bfloat16 [2048, 2048], P('tp'), may hold values from -0.125 to 0.125
- residual_input: bfloat16 [2048, 2048], P(('sp', 'tp')), may hold values from -6 to 6
- attention_norm_gain: float32 [2048], replicated, may hold values from 0.1 to 1.9
- expert_before_gain: float32 [2048], replicated, may hold values from 0.1 to 1.9
- expert_after_gain: float32 [2048], replicated, may hold values from 0.1 to 1.9
- expert_gate_weight: bfloat16 [8, 2048, 4096], P('sp', None, 'tp'), may hold values from -0.125 to 0.125
- expert_up_weight: bfloat16 [8, 2048, 4096], P('sp', None, 'tp'), may hold values from -0.125 to 0.125
- expert_down_weight: bfloat16 [8, 4096, 2048], P('sp', 'tp'), may hold values from -0.09375 to 0.09375
- token_expert_index: int32 [2048, 2], P('sp'), may hold values from 0 to 7, as said below
- routing_weight_matrix: float32 [2048, 2], P('sp'), may hold values from 0.1 to 1
Outputs:
- layer_out: bfloat16 [2048, 2048], P(('sp', 'tp'))
Inputs may be any that keep to these rules, and one draw needn't show every extreme that they name: `token_expert_index`: the 2 experts of a token differ and lie in one group: they have the same value of e // 4. In each aligned block of 256 rows (the rows of one index of sp) no expert is named by more than 80 rows, and the 4 experts of one group are each named by exactly 80 rows in every block.
All inputs are finite; a program needn't handle non-finite values.
Results may differ from a plain program's by a relative error of at most 0.024.
Values may be sent and summed in bfloat16 or wider, within the bound.
A program may use at most 64 MiB of HBM per device.

v0:
```python
import functools

import jax
import jax.numpy as jnp
from jax import lax
from jax.experimental import pallas as pl
from jax.experimental.pallas import tpu as pltpu
from jax.sharding import PartitionSpec as P

KEY_CHANNELS = 64
DV = 128
TOP = 2
BLOCK = 64

EPSILON = 1e-06
DECAY_NORMALIZER = 16.0
HIGHEST = lax.Precision.HIGHEST
MESH = pl.DeviceIdType.MESH
F32 = jnp.float32
BF16 = jnp.bfloat16
FADE_ROWS = 16


def rms_scale(values, gain_row):
    return (
        values * lax.rsqrt(jnp.mean(values * values, axis=-1, keepdims=True) + EPSILON) * gain_row
    )


def contract(a, b, da, db):
    return lax.dot_general(a, b, (((da,), (db,)), ((), ())), preferred_element_type=F32)


def loop(count, body):
    def step(i, carry):
        body(i)
        return carry

    lax.fori_loop(0, count, step, 0)


def remote(src, dst, send, recv, device):
    return pltpu.make_async_remote_copy(
        src_ref=src,
        dst_ref=dst,
        send_sem=send,
        recv_sem=recv,
        device_id=device,
        device_id_type=MESH,
    )


def attention_kernel(
    n_sp, q_hbm, k_hbm, v_hbm, g_hbm, d_hbm, bias_ref, extra_ref, hgain_ref, w_hbm,
    out_ref, message, inbox, carried, gated, q_ref, k_ref, v_ref, g_ref, d_ref, w_ref,
    send_sem, recv_sem, load_sem,
):
    me = lax.axis_index("sp")
    loads = [
        pltpu.make_async_copy(src, dst, load_sem.at[n])
        for n, (src, dst) in enumerate(
            (
                (d_hbm, d_ref),
                (k_hbm, k_ref),
                (v_hbm, v_ref),
                (q_hbm, q_ref),
                (g_hbm, g_ref),
                (w_hbm, w_ref),
            )
        )
    ]
    for copy in loads:
        copy.start()
    barrier = pltpu.get_barrier_semaphore()

    def greet(i):
        @pl.when(me - 1 - i >= 0)
        def _():
            pl.semaphore_signal(
                barrier, inc=1, device_id={"sp": jnp.maximum(me - 1 - i, 0)}, device_id_type=MESH
            )

    loop(n_sp - 1, greet)

    loads[0].wait()
    length, width = q_ref.shape
    heads = width // KEY_CHANNELS
    blocks = length // BLOCK
    x = d_ref[...].astype(F32) + bias_ref[...]
    log_decay = (jnp.minimum(x, 0.0) - jnp.log1p(jnp.exp(-jnp.abs(x)))) / DECAY_NORMALIZER
    extra = extra_ref[...]
    log_decay = log_decay + jnp.concatenate(
        [jnp.broadcast_to(extra[:, h : h + 1], (length, KEY_CHANNELS)) for h in range(heads)],
        axis=1,
    )
    row = lax.broadcasted_iota(jnp.int32, (length, length), 0)
    col = lax.broadcasted_iota(jnp.int32, (length, length), 1)
    causal = (row >= col) & (row // BLOCK == col // BLOCK)
    inside = jnp.dot(
        jnp.where(causal, 1.0, 0.0).astype(F32), log_decay, precision=HIGHEST,
        preferred_element_type=F32,
    )
    ends = [inside[(b + 1) * BLOCK - 1 : (b + 1) * BLOCK, :] for b in range(blocks)]
    offsets = [jnp.zeros_like(ends[0])]
    for b in range(blocks):
        offsets.append(offsets[-1] + ends[b])

    def spread(rows):
        return jnp.concatenate([jnp.broadcast_to(r, (BLOCK, width)) for r in rows], axis=0)

    for copy in loads[1:4]:
        copy.wait()
    q = q_ref[...].astype(F32) * KEY_CHANNELS ** (-0.5)
    k = k_ref[...].astype(F32)
    k_end = (k * jnp.exp(spread(ends) - inside)).astype(BF16)
    states = [jnp.zeros((DV, width), F32)]
    for b in range(blocks):
        rows = slice(b * BLOCK, (b + 1) * BLOCK)
        grown = jnp.concatenate(
            [
                contract(
                    v_ref[rows, h * DV : (h + 1) * DV],
                    k_end[rows, h * KEY_CHANNELS : (h + 1) * KEY_CHANNELS],
                    0,
                    0,
                )
                for h in range(heads)
            ],
            axis=1,
        )
        states.append(states[-1] * jnp.exp(ends[b]) + grown)
    message[0:DV, :] = states[-1].astype(BF16)
    message[DV:, :] = jnp.broadcast_to(jnp.exp(offsets[-1]), (FADE_ROWS, width)).astype(BF16)

    @pl.when(me < n_sp - 1)
    def _():
        pl.semaphore_wait(barrier, n_sp - 1 - me)

    def copy_of(i):
        return remote(
            message, inbox.at[me], send_sem.at[i], recv_sem.at[me],
            {"sp": jnp.minimum(me + 1 + i, n_sp - 1)},
        )

    def send(i):
        @pl.when(me + 1 + i < n_sp)
        def _():
            copy_of(i).start()

    loop(n_sp - 1, send)

    q_in = (q * jnp.exp(inside)).astype(BF16)
    k_inv = (k * jnp.exp(-inside)).astype(BF16)
    q_all = (q * jnp.exp(inside + spread(offsets[:-1]))).astype(BF16)
    local = []
    for h in range(heads):
        cs = slice(h * KEY_CHANNELS, (h + 1) * KEY_CHANNELS)
        scores = jnp.where(causal, contract(q_in[:, cs], k_inv[:, cs], 1, 1), 0.0).astype(BF16)
        within = jnp.dot(scores, v_ref[:, h * DV : (h + 1) * DV], preferred_element_type=F32)
        across = jnp.concatenate(
            [jnp.zeros((BLOCK, DV), F32)]
            + [
                contract(
                    q_in[b * BLOCK : (b + 1) * BLOCK, cs], states[b][:, cs].astype(BF16), 1, 1
                )
                for b in range(1, blocks)
            ],
            axis=0,
        )
        local.append(within + across)

    carried[...] = jnp.zeros_like(carried)

    def take(hop):
        @pl.when(hop < me)
        def _():
            remote(
                message, inbox.at[hop], send_sem.at[0], recv_sem.at[hop], {"sp": me}
            ).wait_recv()
            carried[...] = carried[...] * inbox[hop, DV : DV + 1, :].astype(F32) + inbox[
                hop, 0:DV, :
            ].astype(F32)

    loop(n_sp - 1, take)

    for copy in loads[4:]:
        copy.wait()
    start = carried[...].astype(BF16)
    for h in range(heads):
        cs = slice(h * KEY_CHANNELS, (h + 1) * KEY_CHANNELS)
        vs = slice(h * DV, (h + 1) * DV)
        attn = local[h] + contract(q_all[:, cs], start[:, cs], 1, 1)
        gate = g_ref[:, vs].astype(F32)
        gated[:, vs] = (rms_scale(attn, hgain_ref[...]) * (gate * jax.nn.sigmoid(gate))).astype(
            BF16
        )
    out_ref[...] = jnp.dot(gated[...], w_ref[...], preferred_element_type=F32).astype(BF16)

    def drain(i):
        @pl.when(me + 1 + i < n_sp)
        def _():
            copy_of(i).wait_send()

    loop(n_sp - 1, drain)


def greet_all(n_sp, n_tp, me, j):
    barrier = pltpu.get_barrier_semaphore()

    def along_sp(i):
        pl.semaphore_signal(
            barrier, inc=1, device_id={"sp": lax.rem(me + 1 + i, n_sp)}, device_id_type=MESH
        )

    def along_tp(i):
        pl.semaphore_signal(
            barrier, inc=1, device_id={"tp": lax.rem(j + 1 + i, n_tp)}, device_id_type=MESH
        )

    loop(n_sp - 1, along_sp)
    loop(n_tp - 1, along_tp)
    pl.semaphore_wait(barrier, n_sp + n_tp - 2)


def flipped(me, i, n):
    total, bit = 0, 1
    while bit < n:
        total = total + lax.rem(me // bit + i // bit, 2) * bit
        bit *= 2
    return total


def expert_kernel(
    n_sp, n_tp, cap, part_ref, res_hbm, again_ref, bgain_ref, fgain_ref, target_ref, turned_ref,
    weight_ref, wg_hbm, wu_hbm, wd_hbm,
    out_ref,
    res_ref, wg, wu, wd, ra, rb, tb, normed, xcol, outgoing, rows_ref, hidden, p_ref,
    r1, r2, ty, ob, back, branch, brow, mid_ref,
    load, sa, va, sb, vb, st, vt, ss, vs, sy, vy, sd, vd, s1, v1, s2, v2, s3, v3, s4, v4,
):
    me = lax.axis_index("sp")
    j = lax.axis_index("tp")
    n_y = n_tp // 2
    y, c = j // 2, lax.rem(j, 2)
    sibling = 2 * y + 1 - c
    rows, model = res_ref.shape
    share = model // n_tp
    half = n_sp // 2
    loads = [
        pltpu.make_async_copy(src, dst, load.at[n])
        for n, (src, dst) in enumerate(
            ((res_hbm, res_ref), (wg_hbm, wg), (wu_hbm, wu), (wd_hbm, wd))
        )
    ]
    for copy in loads:
        copy.start()
    greet_all(n_sp, n_tp, me, j)

    def rows_of(index):
        return pl.ds(pl.multiple_of(index * rows, rows), rows)

    def cols_of(index):
        return pl.ds(pl.multiple_of(index * share, share), share)

    def y_at(i):
        return lax.rem(y + 1 + i, n_y)

    def y_from(i):
        return lax.rem(y + n_y - 1 - i, n_y)

    def peer_of(i):
        return flipped(me, i, n_sp)

    def head_pair(i):
        return remote(
            part_ref.at[rows_of(2 * y_at(i) + 1 - c)], ra.at[i], sa.at[i], va.at[i],
            {"tp": sibling},
        )

    def head_far(i):
        return remote(tb.at[i], rb.at[i], sb.at[i], vb.at[i], {"tp": 2 * y_at(i) + c})

    loop(n_y, lambda i: head_pair(i).start())

    def pair_sum(i):
        head_pair(i).wait_recv()
        tb[i] = (
            part_ref[rows_of(2 * y_at(i) + c), :].astype(F32) + ra[i].astype(F32)
        ).astype(BF16)
        head_far(i).start()

    loop(n_y - 1, pair_sum)
    head_pair(n_y - 1).wait_recv()
    mixed = part_ref[rows_of(j), :].astype(F32) + ra[n_y - 1].astype(F32)
    loads[0].wait()
    for i in range(n_y - 1):
        head_far(i).wait_recv()
        mixed = mixed + rb[i].astype(F32)
    mid = (res_ref[...].astype(F32) + rms_scale(mixed, again_ref[...])).astype(BF16)
    mid_ref[...] = mid
    normed[...] = rms_scale(mid.astype(F32), bgain_ref[...]).astype(BF16)

    def turn_copy(i):
        peer = lax.rem(j + 1 + i, n_tp)
        return remote(
            normed.at[:, cols_of(peer)], xcol.at[rows_of(j)], st.at[i], vt.at[i], {"tp": peer}
        )

    loop(n_tp - 1, lambda i: turn_copy(i).start())
    xcol[rows_of(j), :] = normed[:, cols_of(j)]
    loop(n_tp - 1, lambda i: turn_copy(i).wait_recv())

    x = xcol[...]
    t0, t1 = turned_ref[0:1, :], turned_ref[1:2, :]
    tokens = x.shape[0]

    def picked(expert):
        slot = lax.broadcasted_iota(jnp.int32, (cap, tokens), 0) + expert * cap
        chosen = jnp.where((slot == t0) | (slot == t1), 1.0, 0.0).astype(BF16)
        return jnp.dot(chosen, x, preferred_element_type=F32).astype(BF16)

    def out_copy(i):
        return remote(
            outgoing.at[i], rows_ref.at[me, :, cols_of(j)], ss.at[i], vs.at[i],
            {"sp": peer_of(i)},
        )

    def send(i):
        outgoing[i + 1] = picked(peer_of(i + 1))
        out_copy(i + 1).start()

    loop(n_sp - 1, send)
    rows_ref[me, :, cols_of(j)] = picked(me)

    def y_copy(i, m):
        place = rows_ref.at[peer_of(i), :, cols_of(j)]
        return remote(place, place, sy.at[m, i], vy.at[m, i], {"tp": 2 * y_at(m) + c})

    def pair_forward(i, m, owner):
        place = rows_ref.at[peer_of(i), :, cols_of(owner)]
        return remote(place, place, sd.at[m, i], vd.at[m, i], {"tp": sibling})

    def forward(i):
        for m in range(n_y - 1):
            y_copy(i, m).start()
        pair_forward(i, n_y - 1, j).start()

    def arrived(i):
        out_copy(i).wait_recv()
        forward(i)

    def relay(i):
        for m in range(n_y - 1):
            y_copy(i, m).wait_recv()
            pair_forward(i, m, 2 * y_from(m) + c).start()

    def ready(i):
        for m in range(n_y - 1):
            pair_forward(i, m, 2 * y_from(m) + c).wait_recv()
        pair_forward(i, n_y - 1, j).wait_recv()

    def part_pair(i, m):
        return remote(
            p_ref.at[peer_of(i), :, cols_of(2 * y_at(m) + 1 - c)], r1.at[i, m],
            s1.at[i, m], v1.at[i, m], {"tp": sibling},
        )

    def part_far(i, m):
        return remote(
            ty.at[i, m], r2.at[i, m], s2.at[i, m], v2.at[i, m], {"tp": 2 * y_at(m) + c}
        )

    def back_copy(i):
        return remote(ob.at[i], back.at[me], s3.at[i], v3.at[i], {"sp": peer_of(i)})

    def pass_along(i, m):
        part_pair(i, m).wait_recv()
        ty[i, m] = (
            p_ref[peer_of(i), :, cols_of(2 * y_at(m) + c)].astype(F32) + r1[i, m].astype(F32)
        ).astype(BF16)
        part_far(i, m).start()

    def summed(i):
        part_pair(i, n_y - 1).wait_recv()
        total = p_ref[peer_of(i), :, cols_of(j)].astype(F32) + r1[i, n_y - 1].astype(F32)
        for m in range(n_y - 1):
            part_far(i, m).wait_recv()
            total = total + r2[i, m].astype(F32)
        return total.astype(BF16)

    def give_back(i):
        ob[i] = summed(i)
        back_copy(i).start()

    tile = min(256, wg.shape[1])
    steps = wg.shape[1] // tile

    def run_expert(first, during_up, during_down):
        blocks = pl.ds(peer_of(first) // half * half, half)
        batch = half * cap

        def up(t):
            cols = pl.ds(pl.multiple_of(t * tile, tile), tile)
            fed = rows_ref[blocks].reshape(batch, model)
            gate = jnp.dot(fed, wg[:, cols], preferred_element_type=F32)
            rise = jnp.dot(fed, wu[:, cols], preferred_element_type=F32)
            hidden[:, cols] = (gate * jax.nn.sigmoid(gate) * rise).astype(BF16)
            during_up(t)

        loop(steps, up)

        def down(owner):
            made = jnp.dot(hidden[...], wd[:, cols_of(owner)], preferred_element_type=F32)
            p_ref[blocks, :, cols_of(owner)] = made.astype(BF16).reshape(half, cap, share)

        def down_pair(m):
            down(2 * y_at(m) + 1 - c)
            loop(half, lambda i: part_pair(first + i, m).start())
            during_down(m)
            down(2 * y_at(m) + c)

            @pl.when(m < n_y - 1)
            def _():
                loop(half, lambda i: pass_along(first + i, m))

        loop(n_y, down_pair)

    def spaced(count, parts, body):
        each = -(-count // parts)

        def hook(t):
            def one(i):
                @pl.when(t * each + i < count)
                def _():
                    body(jnp.minimum(t * each + i, count - 1))

            loop(each, one)

        return hook

    forward(0)
    loop(half - 1, lambda i: arrived(i + 1))
    loop(half, relay)
    loop(half, ready)
    for copy in loads[1:]:
        copy.wait()
    run_expert(
        0,
        spaced(half, steps, lambda i: arrived(half + i)),
        spaced(half, n_y, lambda i: relay(half + i)),
    )
    loop(half, lambda i: ready(half + i))
    run_expert(
        half,
        spaced(half - 1, steps, lambda i: give_back(i + 1)),
        lambda m: None,
    )
    loop(half, lambda i: give_back(half + i))
    back[me] = summed(0)

    u0, u1 = target_ref[:, 0:1], target_ref[:, 1:2]
    w0, w1 = weight_ref[:, 0:1], weight_ref[:, 1:2]

    def weighed(expert):
        slot = lax.broadcasted_iota(jnp.int32, (tokens, cap), 1) + expert * cap
        mix = jnp.where(slot == u0, w0, 0.0) + jnp.where(slot == u1, w1, 0.0)
        high = mix.astype(BF16)
        low = (mix - high.astype(F32)).astype(BF16)
        served = back[expert]
        return jnp.dot(high, served, preferred_element_type=F32) + jnp.dot(
            low, served, preferred_element_type=F32
        )

    def gather(i, total):
        back_copy(i).wait_recv()
        return total + weighed(peer_of(i))

    branch[...] = lax.fori_loop(1, n_sp, gather, weighed(me)).astype(BF16)

    def home_copy(i):
        peer = lax.rem(j + 1 + i, n_tp)
        return remote(
            branch.at[rows_of(peer)], brow.at[:, cols_of(j)], s4.at[i], v4.at[i], {"tp": peer}
        )

    loop(n_tp - 1, lambda i: home_copy(i).start())
    brow[:, cols_of(j)] = branch[rows_of(j), :]
    loop(n_tp - 1, lambda i: home_copy(i).wait_recv())
    out_ref[...] = (
        mid_ref[...].astype(F32) + rms_scale(brow[...].astype(F32), fgain_ref[...])
    ).astype(BF16)

    loop(n_y, lambda i: head_pair(i).wait_send())
    loop(n_y - 1, lambda i: head_far(i).wait_send())
    loop(n_sp - 1, lambda i: out_copy(i + 1).wait_send())
    loop(n_sp - 1, lambda i: back_copy(i + 1).wait_send())

    def drain_turns(i):
        turn_copy(i).wait_send()
        home_copy(i).wait_send()

    loop(n_tp - 1, drain_turns)

    def drain(i):
        for m in range(n_y - 1):
            y_copy(i, m).wait_send()
            pair_forward(i, m, 2 * y_from(m) + c).wait_send()
            part_far(i, m).wait_send()
        pair_forward(i, n_y - 1, j).wait_send()
        for m in range(n_y):
            part_pair(i, m).wait_send()

    loop(n_sp, drain)


def call(kernel, operands, far, outs, scratch, ident, limit):
    vmem = pl.BlockSpec(memory_space=pltpu.VMEM)
    return pl.pallas_call(
        kernel,
        out_shape=outs,
        in_specs=[
            pl.BlockSpec(memory_space=pl.ANY) if n in far else vmem for n in range(len(operands))
        ],
        out_specs=jax.tree.map(lambda _: vmem, outs),
        scratch_shapes=scratch,
        compiler_params=pltpu.CompilerParams(
            collective_id=ident, has_side_effects=True, vmem_limit_bytes=limit
        ),
    )(*operands)


def dmas(*shapes):
    return [pltpu.SemaphoreType.DMA(s) for s in shapes]


def shards(
    n_sp,
    n_tp,
    query_matrix,
    key_matrix,
    value_matrix,
    output_gate_rows,
    decay_preactivation,
    channel_decay_bias,
    extra_log_decay,
    head_norm_gain,
    output_projection,
    residual_input,
    attention_norm_gain,
    expert_before_gain,
    expert_after_gain,
    expert_gate_weight,
    expert_up_weight,
    expert_down_weight,
    token_expert_index,
    routing_weight_matrix,
):
    length, width = query_matrix.shape
    model = output_projection.shape[1]
    rows = residual_input.shape[0]
    share = model // n_tp
    n_y = n_tp // 2
    capacity = 5 * length // (2 * n_sp)
    cap = (capacity + 15) // 16 * 16
    values = value_matrix.shape[1]

    flat = token_expert_index.reshape(length * TOP)
    one_hot = flat[:, None] == jnp.arange(n_sp, dtype=jnp.int32)[None, :]
    order = jnp.arange(length * TOP, dtype=jnp.int32)
    earlier = (order[:, None] > order[None, :]).astype(BF16)
    counts = jnp.dot(earlier, one_hot.astype(BF16), preferred_element_type=F32)
    slot = jnp.sum(jnp.where(one_hot, counts, 0.0), axis=1).astype(jnp.int32)
    target = (flat * cap + slot).reshape(length, TOP)

    part = call(
        functools.partial(attention_kernel, n_sp),
        (
            query_matrix,
            key_matrix,
            value_matrix,
            output_gate_rows,
            decay_preactivation,
            channel_decay_bias.reshape(1, width),
            extra_log_decay,
            head_norm_gain.reshape(1, DV),
            output_projection,
        ),
        (0, 1, 2, 3, 4, 8),
        jax.ShapeDtypeStruct((length, model), BF16),
        [
            pltpu.VMEM((DV + FADE_ROWS, width), BF16),
            pltpu.VMEM((n_sp, DV + FADE_ROWS, width), BF16),
            pltpu.VMEM((DV, width), F32),
            pltpu.VMEM((length, values), BF16),
            pltpu.VMEM((length, width), BF16),
            pltpu.VMEM((length, width), BF16),
            pltpu.VMEM((length, values), BF16),
            pltpu.VMEM((length, values), BF16),
            pltpu.VMEM((length, width), BF16),
            pltpu.VMEM((values, model), BF16),
        ]
        + dmas((n_sp,), (n_sp,), (6,)),
        1,
        67043328,
    )
    hidden_units = expert_gate_weight.shape[2]
    by_peer = (n_sp, n_y)
    return call(
        functools.partial(expert_kernel, n_sp, n_tp, cap),
        (
            part,
            residual_input,
            attention_norm_gain.reshape(1, model),
            expert_before_gain.reshape(1, model),
            expert_after_gain.reshape(1, model),
            target,
            target.T,
            routing_weight_matrix,
            expert_gate_weight[0],
            expert_up_weight[0],
            expert_down_weight[0],
        ),
        (1, 8, 9, 10),
        jax.ShapeDtypeStruct((rows, model), BF16),
        [
            pltpu.VMEM((rows, model), BF16),
            pltpu.VMEM((model, hidden_units), BF16),
            pltpu.VMEM((model, hidden_units), BF16),
            pltpu.VMEM((hidden_units, model), BF16),
            pltpu.VMEM((n_y, rows, model), BF16),
            pltpu.VMEM((n_y, rows, model), BF16),
            pltpu.VMEM((n_y, rows, model), BF16),
            pltpu.VMEM((rows, model), BF16),
            pltpu.VMEM((length, share), BF16),
            pltpu.VMEM((n_sp, cap, share), BF16),
            pltpu.VMEM((n_sp, cap, model), BF16),
            pltpu.VMEM((n_sp // 2 * cap, hidden_units), BF16),
            pltpu.VMEM((n_sp, cap, model), BF16),
            pltpu.VMEM(by_peer + (cap, share), BF16),
            pltpu.VMEM(by_peer + (cap, share), BF16),
            pltpu.VMEM(by_peer + (cap, share), BF16),
            pltpu.VMEM((n_sp, cap, share), BF16),
            pltpu.VMEM((n_sp, cap, share), BF16),
            pltpu.VMEM((length, share), BF16),
            pltpu.VMEM((rows, model), BF16),
            pltpu.VMEM((rows, model), BF16),
        ]
        + dmas(
            (4,), (n_y,), (n_y,), (n_y,), (n_y,), (n_tp,), (n_tp,), (n_sp,), (n_sp,),
            (n_y, n_sp), (n_y, n_sp), (n_y, n_sp), (n_y, n_sp),
            by_peer, by_peer, by_peer, by_peer, (n_sp,), (n_sp,), (n_tp,), (n_tp,),
        ),
        2,
        67043328,
    )


def solution(mesh):
    placed = (
        P("sp", "tp"),
        P("sp", "tp"),
        P("sp", "tp"),
        P("sp", "tp"),
        P("sp", "tp"),
        P("tp"),
        P("sp", "tp"),
        P(),
        P("tp", None),
        P(("sp", "tp"), None),
        P(),
        P(),
        P(),
        P("sp", None, "tp"),
        P("sp", None, "tp"),
        P("sp", "tp", None),
        P("sp", None),
        P("sp", None),
    )
    return jax.shard_map(
        functools.partial(shards, mesh.shape["sp"], mesh.shape["tp"]),
        mesh=mesh,
        in_specs=placed,
        out_specs=P(("sp", "tp"), None),
        check_vma=False,
    )
```

profile of v0, /device:TPU:0, one launch (start us, length us, event | category | flops | bytes accessed | tf_op | source)
XLA Modules:
  0.0 103.5 jit_solution(15299354073143943389)
XLA Ops:
  0.0 1.5 %copy.22.extra_ref = f32[256,4]{1,0:T(8,128)} copy(f32[256,4]{0,1:T(4,128)} %param.24) | data formatting | bytes 8192 | tf_op args[6]
  1.5 1.5 %copy.26.weight_ref = f32[256,2]{1,0:T(8,128)} copy(f32[256,2]{0,1:T(2,128)} %param.35) | data formatting | bytes 4096 | tf_op args[17]
  3.0 0.8 copy.23
  3.8 0.1 eq.15
  3.9 0.3 fusion
  4.2 0.1 convert_element_type.10
  4.3 0.1 copy.24
  4.4 0.7 multiply_add_fusion
  5.1 0.0 copy-start
  5.1 0.6 copy-done
  5.7 0.8 copy.25.target_ref
  6.5 17.6 %shard_map.172.part_ref = bf16[256,2048]{1,0:T(8,128)(2,1)} custom-call(bf16[256,256]{1,0:T(8,128)(2,1)} %q_hbm.1, bf16[256,256]{1,0:T(8,128)(2,1)} %k_hbm.1, bf16[256,512]{1,0:T(8,128)(2,1)} %v_hbm.1, bf16[256,512]{1,0:T(8,128)(2,1)} %g_hbm.1, bf16[256,256]{1,0:T(8,128)(2,1)} %d_hbm.1, f32[1,256]{1,0:T(1,128)} %bitcast.16, f32[256,4]{1,0:T(8,128)} %copy.22.extra_ref, ...), custom_call_target="tpu_custom_call" | custom-call | tf_op jit(solution)/shard_map/pallas_call | solution.py:518
  24.1 77.8 %shard_map.173 = bf16[64,2048]{1,0:T(8,128)(2,1)} custom-call(bf16[256,2048]{1,0:T(8,128)(2,1)} %shard_map.172.part_ref, bf16[64,2048]{1,0:T(8,128)(2,1)} %res_hbm.1, f32[1,2048]{1,0:T(1,128)} %bitcast.13, f32[1,2048]{1,0:T(1,128)} %bitcast.14, f32[1,2048]{1,0:T(1,128)} %bitcast.15, s32[256,2]{1,0:T(8,128)} %copy.25.target_ref, s32[2,256]{1,0:T(2,128)} %bitcast.12, ...), custom_call_target="tpu_custom_call" | custom-call | tf_op jit(solution)/shard_map/pallas_call | solution.py:518
  101.9 1.7 %copy.28 = bf16[64,2048]{1,0:T(8,128)(2,1)} copy(bf16[64,2048]{1,0:T(8,128)(2,1)} %shard_map.173) | data formatting | bytes 524288
  (1 shorter events, 0.0 us)
Async XLA Ops:
  5.1 0.6 copy-start
where the time goes:
time: 105 us; the launch traced here: 104 us
  Pallas kernels  95.4 us (91%)
  local copies, waits for them, and re-layouts  7.15 us (7%)
    pallas_call x2, Pallas kernels, call(): pl.pallas_call(kernel, out_shape=outs, in_specs=[pl.BlockSpec(memory_spac...  95.4 us
    unnamed x6, local copies, waits for them, and re-layouts  6 us

commit v1 on v0

v1 whole, which is shorter than its diff:
```python
import contextlib
import functools

import jax
import jax.numpy as jnp
from jax import lax
from jax.experimental import pallas as pl
from jax.experimental.pallas import tpu as pltpu
from jax.sharding import PartitionSpec as P

KEY_CHANNELS = 64
DV = 128
TOP = 2
BLOCK = 64

EPSILON = 1e-06
DECAY_NORMALIZER = 16.0
HIGHEST = lax.Precision.HIGHEST
MESH = pl.DeviceIdType.MESH
F32 = jnp.float32
BF16 = jnp.bfloat16
FADE_ROWS = 16
PARTS = 4
TILE = 512
VMEM_LIMIT = 67043328


def scope(name):
    return contextlib.nullcontext()


def rms_scale(values, gain_row):
    return (
        values * lax.rsqrt(jnp.mean(values * values, axis=-1, keepdims=True) + EPSILON) * gain_row
    )


def contract(a, b, da, db):
    return lax.dot_general(a, b, (((da,), (db,)), ((), ())), preferred_element_type=F32)


def loop(count, body):
    def step(i, carry):
        body(i)
        return carry

    lax.fori_loop(0, count, step, 0)


def remote(src, dst, send, recv, device):
    return pltpu.make_async_remote_copy(
        src_ref=src,
        dst_ref=dst,
        send_sem=send,
        recv_sem=recv,
        device_id=device,
        device_id_type=MESH,
    )


def flipped(me, i, n):
    total, bit = 0, 1
    while bit < n:
        total = total + lax.rem(me // bit + i // bit, 2) * bit
        bit *= 2
    return total


def thirds(values):
    high = values.astype(BF16)
    rest = values - high.astype(F32)
    mid = rest.astype(BF16)
    return high, mid, (rest - mid.astype(F32)).astype(BF16)


def unit_order(n_sp):
    half = n_sp // 2
    pairs = [(i, 2) for i in range(0, half, 2)]
    singles = [(i, 1) for i in range(half, n_sp)]
    units = []
    while pairs or singles:
        if pairs:
            units.append(pairs.pop(0))
        if singles:
            units.append(singles.pop(0))
    return units


def layer_kernel(
    n_sp, n_tp, cap,
    d_hbm, bias_hbm, extra_hbm, k_hbm, v_hbm, q_hbm, g_hbm, hgain_hbm, index_hbm, weight_hbm,
    w_hbm, res_hbm, again_hbm, bgain_hbm, fgain_hbm, wg_hbm, wu_hbm, wd_hbm,
    out_ref,
    d_ref, bias_ref, extra_ref, k_ref, v_ref, q_ref, g_ref, hgain_ref, index_ref, weight_ref,
    w_ref, res_ref, again_ref, bgain_ref, fgain_ref, wg, wu, wd,
    message, pairbox, zmsg, inbox, carried, exch_out, exch_in, gated, part_ref, mixed_ref,
    ra, rb, tb, normed, xcol, sel_ref, mix_ref, outgoing, rows_ref, hidden, p_ref,
    r1, r2, ty, ob, back, acc, branch, brow, mid_ref,
    load, s_pair, r_pair, s_z, r_z,
    sa, va, sb, vb, st, vt, ss, vs, sy, vy, sd, vd, s1, v1, s2, v2, s3, v3, s4, v4,
):
    me = lax.axis_index("sp")
    j = lax.axis_index("tp")
    loads = [
        pltpu.make_async_copy(src, dst, load.at[n])
        for n, (src, dst) in enumerate(
            (
                (d_hbm, d_ref),
                (bias_hbm, bias_ref),
                (extra_hbm, extra_ref),
                (k_hbm, k_ref),
                (v_hbm, v_ref),
                (q_hbm, q_ref),
                (g_hbm, g_ref),
                (hgain_hbm, hgain_ref),
                (index_hbm, index_ref),
                (weight_hbm, weight_ref),
                (w_hbm, w_ref),
                (res_hbm, res_ref),
                (again_hbm, again_ref),
                (bgain_hbm, bgain_ref),
                (fgain_hbm, fgain_ref),
                (wg_hbm, wg),
                (wu_hbm, wu),
                (wd_hbm, wd),
            )
        )
    ]
    for copy in loads:
        copy.start()
    barrier = pltpu.get_barrier_semaphore()

    def along_sp(i):
        pl.semaphore_signal(
            barrier, inc=1, device_id={"sp": lax.rem(me + 1 + i, n_sp)}, device_id_type=MESH
        )

    def along_tp(i):
        pl.semaphore_signal(
            barrier, inc=1, device_id={"tp": lax.rem(j + 1 + i, n_tp)}, device_id_type=MESH
        )

    loop(n_sp - 1, along_sp)
    loop(n_tp - 1, along_tp)

    side = lax.rem(me, 2)
    pair = me // 2
    n_pair = n_sp // 2
    partner = me + 1 - 2 * side
    n_y = n_tp // 2
    y, c = j // 2, lax.rem(j, 2)
    sibling = 2 * y + 1 - c
    length, width = q_ref.shape
    rows, model = res_ref.shape
    share = model // n_tp
    half = n_sp // 2
    heads = width // KEY_CHANNELS
    blocks = length // BLOCK
    half_width = width // 2

    with scope("a_wait0"):
        for copy in loads[0:3]:
            copy.wait()
    with scope("a_decay"):
        x = d_ref[...].astype(F32) + bias_ref[...]
        log_decay = (jnp.minimum(x, 0.0) - jnp.log1p(jnp.exp(-jnp.abs(x)))) / DECAY_NORMALIZER
        row = lax.broadcasted_iota(jnp.int32, (length, length), 0)
        col = lax.broadcasted_iota(jnp.int32, (length, length), 1)
        causal = (row >= col) & (row // BLOCK == col // BLOCK)
        triangle = jnp.where(causal, 1.0, 0.0).astype(F32)
        ones = triangle.astype(BF16)
        inside = sum(jnp.dot(ones, p, preferred_element_type=F32) for p in thirds(log_decay))
        extra = lax.dot_general(
            triangle, extra_ref[...], (((1,), (1,)), ((), ())), precision=HIGHEST,
            preferred_element_type=F32,
        )
        inside = inside + jnp.concatenate(
            [jnp.broadcast_to(extra[:, h : h + 1], (length, KEY_CHANNELS)) for h in range(heads)],
            axis=1,
        )
    ends = [inside[(b + 1) * BLOCK - 1 : (b + 1) * BLOCK, :] for b in range(blocks)]
    offsets = [jnp.zeros_like(ends[0])]
    for b in range(blocks):
        offsets.append(offsets[-1] + ends[b])

    def spread(pieces):
        return jnp.concatenate([jnp.broadcast_to(r, (BLOCK, width)) for r in pieces], axis=0)

    for copy in loads[3:6]:
        copy.wait()
    with scope("a_state"):
        q = q_ref[...].astype(F32) * KEY_CHANNELS ** (-0.5)
        k = k_ref[...].astype(F32)
        k_end = (k * jnp.exp(spread(ends) - inside)).astype(BF16)
        states = [jnp.zeros((DV, width), F32)]
        for b in range(blocks):
            at = slice(b * BLOCK, (b + 1) * BLOCK)
            grown = jnp.concatenate(
                [
                    contract(
                        v_ref[at, h * DV : (h + 1) * DV],
                        k_end[at, h * KEY_CHANNELS : (h + 1) * KEY_CHANNELS],
                        0,
                        0,
                    )
                    for h in range(heads)
                ],
                axis=1,
            )
            states.append(states[-1] * jnp.exp(ends[b]) + grown)
        fade = jnp.exp(offsets[-1])
        for h in range(2):
            cs = slice(h * half_width, (h + 1) * half_width)
            message[h, 0:DV, :] = states[-1][:, cs].astype(BF16)
            message[h, DV:, :] = jnp.broadcast_to(fade[:, cs], (FADE_ROWS, half_width)).astype(BF16)

    with scope("a_barrier"):
        pl.semaphore_wait(barrier, n_sp + n_tp - 2)
    pair_copy = remote(
        message.at[1 - side], pairbox, s_pair.at[0], r_pair.at[0], {"sp": partner}
    )
    pair_copy.start()

    with scope("a_local"):
        q_in = (q * jnp.exp(inside)).astype(BF16)
        k_inv = (k * jnp.exp(-inside)).astype(BF16)
        q_all = (q * jnp.exp(inside + spread(offsets[:-1]))).astype(BF16)
        local = []
        for h in range(heads):
            cs = slice(h * KEY_CHANNELS, (h + 1) * KEY_CHANNELS)
            scores = jnp.where(causal, contract(q_in[:, cs], k_inv[:, cs], 1, 1), 0.0).astype(BF16)
            within = jnp.dot(scores, v_ref[:, h * DV : (h + 1) * DV], preferred_element_type=F32)
            across = jnp.concatenate(
                [jnp.zeros((BLOCK, DV), F32)]
                + [
                    contract(
                        q_in[b * BLOCK : (b + 1) * BLOCK, cs], states[b][:, cs].astype(BF16), 1, 1
                    )
                    for b in range(1, blocks)
                ],
                axis=0,
            )
            local.append(within + across)

    with scope("a_pair"):
        pair_copy.wait_recv()
        mine = message[side].astype(F32)
        other = pairbox[...].astype(F32)
        first = jnp.where(side == 0, mine, other)
        second = jnp.where(side == 0, other, mine)
        zmsg[0:DV, :] = (first[0:DV] * second[DV : DV + 1] + second[0:DV]).astype(BF16)
        zmsg[DV:, :] = (first[DV:] * second[DV:]).astype(BF16)

    def z_copy(i):
        return remote(
            zmsg, inbox.at[pair], s_z.at[i], r_z.at[pair],
            {"sp": 2 * jnp.minimum(pair + 1 + i, n_pair - 1) + side},
        )

    def z_send(i):
        @pl.when(pair + 1 + i < n_pair)
        def _():
            z_copy(i).start()

    loop(n_pair - 1, z_send)

    def peer_of(i):
        return flipped(me, i, n_sp)

    with scope("a_route"):
        loads[8].wait()
        loads[9].wait()
        e0, e1 = index_ref[0:1, :], index_ref[1:2, :]
        named = lax.broadcasted_iota(jnp.int32, (n_sp, length), 0)
        taken = jnp.where((named == e0) | (named == e1), 1.0, 0.0).astype(BF16)
        before = jnp.where(row < col, 1.0, 0.0).astype(BF16)
        counts = jnp.dot(taken, before, preferred_element_type=F32)

        def target(e):
            place = jnp.sum(jnp.where(named == e, counts, 0.0), axis=0, keepdims=True)
            return e.astype(F32) * cap + place

        t0, t1 = target(e0), target(e1)
        w0, w1 = weight_ref[0:1, :], weight_ref[1:2, :]

        def route(i):
            slot = lax.broadcasted_iota(jnp.int32, (cap, length), 0) + peer_of(i) * cap
            slot = slot.astype(F32)
            is0, is1 = slot == t0, slot == t1
            sel_ref[i] = jnp.where(is0 | is1, 1.0, 0.0).astype(BF16)
            mix_ref[i] = (jnp.where(is0, w0, 0.0) + jnp.where(is1, w1, 0.0)).astype(BF16)

        loop(n_sp, route)

    carried[...] = jnp.zeros_like(carried)

    def take(hop):
        @pl.when(hop < pair)
        def _():
            remote(
                zmsg, inbox.at[hop], s_z.at[0], r_z.at[hop], {"sp": partner}
            ).wait_recv()
            carried[...] = carried[...] * inbox[hop, DV : DV + 1, :].astype(F32) + inbox[
                hop, 0:DV, :
            ].astype(F32)

    with scope("a_take"):
        loop(n_pair - 1, take)

    with scope("a_exch"):
        before_pair = carried[...]
        head = jnp.where(
            side == 0, message[side].astype(F32), pairbox[...].astype(F32)
        )
        after_first = before_pair * head[DV : DV + 1] + head[0:DV]
        own_start = jnp.where(side == 0, before_pair, after_first)
        exch_out[...] = jnp.where(side == 0, after_first, before_pair).astype(BF16)
        exch_copy = remote(exch_out, exch_in, s_pair.at[1], r_pair.at[1], {"sp": partner})
        exch_copy.start()
        exch_copy.wait_recv()
        got = exch_in[...].astype(F32)
        start = jnp.concatenate(
            [jnp.where(side == 0, own_start, got), jnp.where(side == 0, got, own_start)], axis=1
        ).astype(BF16)

    for copy in loads[6:8]:
        copy.wait()
    with scope("a_gate"):
        for h in range(heads):
            cs = slice(h * KEY_CHANNELS, (h + 1) * KEY_CHANNELS)
            at = slice(h * DV, (h + 1) * DV)
            attn = local[h] + contract(q_all[:, cs], start[:, cs], 1, 1)
            gate = g_ref[:, at].astype(F32)
            gated[:, at] = (rms_scale(attn, hgain_ref[...]) * (gate * jax.nn.sigmoid(gate))).astype(
                BF16
            )

    def rows_of(index):
        return pl.ds(pl.multiple_of(index * rows, rows), rows)

    def cols_of(index):
        return pl.ds(pl.multiple_of(index * share, share), share)

    piece = model // PARTS

    def piece_of(q):
        return pl.ds(pl.multiple_of(q * piece, piece), piece)

    def y_at(i):
        return lax.rem(y + 1 + i, n_y)

    def y_from(i):
        return lax.rem(y + n_y - 1 - i, n_y)

    def head_pair(m, q):
        return remote(
            part_ref.at[rows_of(2 * y_at(m) + 1 - c), piece_of(q)], ra.at[m, :, piece_of(q)],
            sa.at[m, q], va.at[m, q], {"tp": sibling},
        )

    def head_far(m, q):
        return remote(
            tb.at[m, :, piece_of(q)], rb.at[m, :, piece_of(q)], sb.at[m, q], vb.at[m, q],
            {"tp": 2 * y_at(m) + c},
        )

    def project(t):
        m, q = t // PARTS, lax.rem(t, PARTS)
        at = pl.ds(pl.multiple_of(2 * y_at(m) * rows, 2 * rows), 2 * rows)
        part_ref[at, piece_of(q)] = jnp.dot(
            gated[at, :], w_ref[:, piece_of(q)], preferred_element_type=F32
        ).astype(BF16)
        head_pair(m, q).start()

    def pair_sum(t):
        m, q = t // PARTS, lax.rem(t, PARTS)
        head_pair(m, q).wait_recv()
        tb[m, :, piece_of(q)] = (
            part_ref[rows_of(2 * y_at(m) + c), piece_of(q)].astype(F32)
            + ra[m, :, piece_of(q)].astype(F32)
        ).astype(BF16)
        head_far(m, q).start()

    def whole_sum(q):
        head_pair(n_y - 1, q).wait_recv()
        total = part_ref[rows_of(j), piece_of(q)].astype(F32) + ra[
            n_y - 1, :, piece_of(q)
        ].astype(F32)
        for m in range(n_y - 1):
            head_far(m, q).wait_recv()
            total = total + rb[m, :, piece_of(q)].astype(F32)
        mixed_ref[:, piece_of(q)] = total

    with scope("e_proj"):
        loads[10].wait()
        loop(n_y * PARTS, project)
    with scope("e_pair"):
        loop((n_y - 1) * PARTS, pair_sum)
    with scope("e_rs"):
        loop(PARTS, whole_sum)
    with scope("e_norm"):
        for copy in loads[11:15]:
            copy.wait()
        mid = (res_ref[...].astype(F32) + rms_scale(mixed_ref[...], again_ref[...])).astype(BF16)
        mid_ref[...] = mid
        normed[...] = rms_scale(mid.astype(F32), bgain_ref[...]).astype(BF16)

    def turn_copy(i):
        peer = lax.rem(j + 1 + i, n_tp)
        return remote(
            normed.at[:, cols_of(peer)], xcol.at[rows_of(j)], st.at[i], vt.at[i], {"tp": peer}
        )

    with scope("e_turn"):
        loop(n_tp - 1, lambda i: turn_copy(i).start())
        xcol[rows_of(j), :] = normed[:, cols_of(j)]
        loop(n_tp - 1, lambda i: turn_copy(i).wait_recv())

    def picked(i):
        return jnp.dot(sel_ref[i], xcol[...], preferred_element_type=F32).astype(BF16)

    def out_copy(i):
        return remote(
            outgoing.at[i], rows_ref.at[i, :, cols_of(j)], ss.at[i], vs.at[i],
            {"sp": peer_of(i)},
        )

    def y_copy(i, m):
        place = rows_ref.at[i, :, cols_of(j)]
        return remote(place, place, sy.at[m, i], vy.at[m, i], {"tp": 2 * y_at(m) + c})

    def pair_forward(i, m, owner):
        place = rows_ref.at[i, :, cols_of(owner)]
        return remote(place, place, sd.at[m, i], vd.at[m, i], {"tp": sibling})

    def forward(i):
        for m in range(n_y - 1):
            y_copy(i, m).start()
        pair_forward(i, n_y - 1, j).start()

    def arrived(i):
        out_copy(i).wait_recv()
        forward(i)

    def relay(i):
        for m in range(n_y - 1):
            y_copy(i, m).wait_recv()
            pair_forward(i, m, 2 * y_from(m) + c).start()

    def ready(i):
        for m in range(n_y - 1):
            pair_forward(i, m, 2 * y_from(m) + c).wait_recv()
        pair_forward(i, n_y - 1, j).wait_recv()

    def part_pair(i, m):
        return remote(
            p_ref.at[i, :, cols_of(2 * y_at(m) + 1 - c)], r1.at[i, m],
            s1.at[i, m], v1.at[i, m], {"tp": sibling},
        )

    def part_far(i, m):
        return remote(
            ty.at[i, m], r2.at[i, m], s2.at[i, m], v2.at[i, m], {"tp": 2 * y_at(m) + c}
        )

    def back_copy(i):
        return remote(ob.at[i], back.at[i], s3.at[i], v3.at[i], {"sp": peer_of(i)})

    def pass_along(i):
        for m in range(n_y - 1):
            part_pair(i, m).wait_recv()
            ty[i, m] = (
                p_ref[i, :, cols_of(2 * y_at(m) + c)].astype(F32) + r1[i, m].astype(F32)
            ).astype(BF16)
            part_far(i, m).start()

    def summed(i):
        part_pair(i, n_y - 1).wait_recv()
        total = p_ref[i, :, cols_of(j)].astype(F32) + r1[i, n_y - 1].astype(F32)
        for m in range(n_y - 1):
            part_far(i, m).wait_recv()
            total = total + r2[i, m].astype(F32)
        return total.astype(BF16)

    def give_back(i):
        if i == 0:
            back[0] = summed(0)
        else:
            ob[i] = summed(i)
            back_copy(i).start()

    tile = min(TILE, wg.shape[1])
    steps = wg.shape[1] // tile

    def run_expert(first, count, after_first_up, after_up, after_first_down):
        batch = count * cap

        def up(t):
            cols = pl.ds(pl.multiple_of(t * tile, tile), tile)
            fed = rows_ref[first : first + count].reshape(batch, model)
            gate = jnp.dot(fed, wg[:, cols], preferred_element_type=F32)
            rise = jnp.dot(fed, wu[:, cols], preferred_element_type=F32)
            hidden[0:batch, cols] = (gate * jax.nn.sigmoid(gate) * rise).astype(BF16)

            @pl.when(t == 0)
            def _():
                after_first_up()

        loop(steps, up)
        after_up()

        def down(owner):
            made = jnp.dot(hidden[0:batch, :], wd[:, cols_of(owner)], preferred_element_type=F32)
            p_ref[first : first + count, :, cols_of(owner)] = made.astype(BF16).reshape(
                count, cap, share
            )

        def down_pair(m):
            down(2 * y_at(m) + 1 - c)
            for i in range(count):
                part_pair(first + i, m).start()
            down(2 * y_at(m) + c)

            @pl.when(m == 0)
            def _():
                after_first_down()

        loop(n_y, down_pair)

    units = unit_order(n_sp)
    total_units = len(units)

    def each(k, body):
        if 0 <= k < total_units:
            for i in range(units[k][0], units[k][0] + units[k][1]):
                body(i)

    def arrive(k):
        each(k, lambda i: arrived(i) if i > 0 else None)

    with scope("e_send"):
        rows_ref[0, :, cols_of(j)] = picked(0)
        forward(0)

        def send(t):
            i = jnp.where(lax.rem(t, 2) == 0, half + t // 2, 1 + t // 2)
            outgoing[i] = picked(i)
            out_copy(i).start()

        loop(n_sp - 1, send)
    with scope("e_arrive"):
        arrive(0)
        relay(0)
        arrive(1)
        arrive(2)
    with scope("e_relay"):
        for i in range(1, units[0][1]):
            relay(i)
    with scope("e_weights"):
        for copy in loads[15:]:
            copy.wait()
    for k, (first, count) in enumerate(units):
        with scope(f"e_ready{k}"):
            each(k, ready)
        with scope(f"e_run{k}"):
            run_expert(
                first,
                count,
                lambda: each(k - 1, pass_along),
                lambda: each(k + 1, relay),
                lambda: each(k - 2, give_back),
            )
        with scope(f"e_arrive{k}"):
            arrive(k + 3)
    with scope("e_give"):
        each(total_units - 1, pass_along)
        each(total_units - 2, give_back)
        each(total_units - 1, give_back)

    def weighed(i):
        return contract(mix_ref[i], back[i], 0, 0)

    with scope("e_gather"):
        acc[...] = weighed(0)

        def gather(t):
            back_copy(t + 1).wait_recv()
            acc[...] = acc[...] + weighed(t + 1)

        loop(n_sp - 2, gather)
        back_copy(n_sp - 1).wait_recv()
        branch[...] = (acc[...] + weighed(n_sp - 1)).astype(BF16)

    def home_copy(i):
        peer = lax.rem(j + 1 + i, n_tp)
        return remote(
            branch.at[rows_of(peer)], brow.at[:, cols_of(j)], s4.at[i], v4.at[i], {"tp": peer}
        )

    with scope("e_home"):
        loop(n_tp - 1, lambda i: home_copy(i).start())
        brow[:, cols_of(j)] = branch[rows_of(j), :]
        loop(n_tp - 1, lambda i: home_copy(i).wait_recv())
    with scope("e_out"):
        out_ref[...] = (
            mid_ref[...].astype(F32) + rms_scale(brow[...].astype(F32), fgain_ref[...])
        ).astype(BF16)

    with scope("e_drain"):
        pair_copy.wait_send()
        exch_copy.wait_send()

        def drain_z(i):
            @pl.when(pair + 1 + i < n_pair)
            def _():
                z_copy(i).wait_send()

        loop(n_pair - 1, drain_z)
        loop(n_y * PARTS, lambda t: head_pair(t // PARTS, lax.rem(t, PARTS)).wait_send())
        loop((n_y - 1) * PARTS, lambda t: head_far(t // PARTS, lax.rem(t, PARTS)).wait_send())

        def drain_sp(i):
            out_copy(i + 1).wait_send()
            back_copy(i + 1).wait_send()

        loop(n_sp - 1, drain_sp)

        def drain_turns(i):
            turn_copy(i).wait_send()
            home_copy(i).wait_send()

        loop(n_tp - 1, drain_turns)

        def drain(i):
            for m in range(n_y - 1):
                y_copy(i, m).wait_send()
                pair_forward(i, m, 2 * y_from(m) + c).wait_send()
                part_far(i, m).wait_send()
            pair_forward(i, n_y - 1, j).wait_send()
            for m in range(n_y):
                part_pair(i, m).wait_send()

        loop(n_sp, drain)


def dmas(*shapes):
    return [pltpu.SemaphoreType.DMA(s) for s in shapes]


def shards(
    n_sp,
    n_tp,
    query_matrix,
    key_matrix,
    value_matrix,
    output_gate_rows,
    decay_preactivation,
    channel_decay_bias,
    extra_log_decay,
    head_norm_gain,
    output_projection,
    residual_input,
    attention_norm_gain,
    expert_before_gain,
    expert_after_gain,
    expert_gate_weight,
    expert_up_weight,
    expert_down_weight,
    token_expert_index,
    routing_weight_matrix,
):
    length, width = query_matrix.shape
    model = output_projection.shape[1]
    rows = residual_input.shape[0]
    share = model // n_tp
    n_y = n_tp // 2
    capacity = 5 * length // (2 * n_sp)
    cap = (capacity + 15) // 16 * 16
    values = value_matrix.shape[1]
    hidden_units = expert_gate_weight.shape[2]
    by_peer = (n_sp, n_y)
    state = (DV + FADE_ROWS, width // 2)

    operands = (
        decay_preactivation,
        channel_decay_bias.reshape(1, width),
        extra_log_decay.T,
        key_matrix,
        value_matrix,
        query_matrix,
        output_gate_rows,
        head_norm_gain.reshape(1, DV),
        token_expert_index.T,
        routing_weight_matrix.T,
        output_projection,
        residual_input,
        attention_norm_gain.reshape(1, model),
        expert_before_gain.reshape(1, model),
        expert_after_gain.reshape(1, model),
        expert_gate_weight[0],
        expert_up_weight[0],
        expert_down_weight[0],
    )
    kept = [pltpu.VMEM(a.shape, a.dtype) for a in operands]
    return pl.pallas_call(
        functools.partial(layer_kernel, n_sp, n_tp, cap),
        out_shape=jax.ShapeDtypeStruct((rows, model), BF16),
        in_specs=[pl.BlockSpec(memory_space=pl.ANY)] * len(operands),
        out_specs=pl.BlockSpec(memory_space=pltpu.VMEM),
        scratch_shapes=kept
        + [
            pltpu.VMEM((2,) + state, BF16),
            pltpu.VMEM(state, BF16),
            pltpu.VMEM(state, BF16),
            pltpu.VMEM((n_sp // 2,) + state, BF16),
            pltpu.VMEM((DV, width // 2), F32),
            pltpu.VMEM((DV, width // 2), BF16),
            pltpu.VMEM((DV, width // 2), BF16),
            pltpu.VMEM((length, values), BF16),
            pltpu.VMEM((length, model), BF16),
            pltpu.VMEM((rows, model), F32),
            pltpu.VMEM((n_y, rows, model), BF16),
            pltpu.VMEM((n_y, rows, model), BF16),
            pltpu.VMEM((n_y, rows, model), BF16),
            pltpu.VMEM((rows, model), BF16),
            pltpu.VMEM((length, share), BF16),
            pltpu.VMEM((n_sp, cap, length), BF16),
            pltpu.VMEM((n_sp, cap, length), BF16),
            pltpu.VMEM((n_sp, cap, share), BF16),
            pltpu.VMEM((n_sp, cap, model), BF16),
            pltpu.VMEM((2 * cap, hidden_units), BF16),
            pltpu.VMEM((n_sp, cap, model), BF16),
            pltpu.VMEM(by_peer + (cap, share), BF16),
            pltpu.VMEM(by_peer + (cap, share), BF16),
            pltpu.VMEM(by_peer + (cap, share), BF16),
            pltpu.VMEM((n_sp, cap, share), BF16),
            pltpu.VMEM((n_sp, cap, share), BF16),
            pltpu.VMEM((length, share), F32),
            pltpu.VMEM((length, share), BF16),
            pltpu.VMEM((rows, model), BF16),
            pltpu.VMEM((rows, model), BF16),
        ]
        + dmas(
            (len(operands),), (2,), (2,), (n_sp // 2,), (n_sp // 2,),
            (n_y, PARTS), (n_y, PARTS), (n_y, PARTS), (n_y, PARTS),
            (n_tp,), (n_tp,), (n_sp,), (n_sp,),
            (n_y, n_sp), (n_y, n_sp), (n_y, n_sp), (n_y, n_sp),
            by_peer, by_peer, by_peer, by_peer, (n_sp,), (n_sp,), (n_tp,), (n_tp,),
        ),
        compiler_params=pltpu.CompilerParams(
            collective_id=1, has_side_effects=True, vmem_limit_bytes=VMEM_LIMIT
        ),
    )(*operands)


def solution(mesh):
    placed = (
        P("sp", "tp"),
        P("sp", "tp"),
        P("sp", "tp"),
        P("sp", "tp"),
        P("sp", "tp"),
        P("tp"),
        P("sp", "tp"),
        P(),
        P("tp", None),
        P(("sp", "tp"), None),
        P(),
        P(),
        P(),
        P("sp", None, "tp"),
        P("sp", None, "tp"),
        P("sp", "tp", None),
        P("sp", None),
        P("sp", None),
    )
    return jax.shard_map(
        functools.partial(shards, mesh.shape["sp"], mesh.shape["tp"]),
        mesh=mesh,
        in_specs=placed,
        out_specs=P(("sp", "tp"), None),
        check_vma=False,
    )
```

time: 105 us -> 86.6 us (0.82)
  Pallas kernels: 95.4 us -> 83.7 us
  local copies, waits for them, and re-layouts: 7.15 us -> 1.67 us
    pallas_call x2 -> x1, Pallas kernels: 95.4 us -> 83.7 us  [shards(): pl.pallas_call(functools.partial(layer_kernel, n_sp, n_tp, cap), out_shap...]
    unnamed x6 -> x1, local copies, waits for them, and re-layouts: 6 us -> 1.67 us
where the time goes in v1:
time: 86.6 us; the launch traced here: 85.4 us
  Pallas kernels  83.7 us (97%)
  local copies, waits for them, and re-layouts  1.67 us (2%)
    pallas_call x1, Pallas kernels, shards(): pl.pallas_call(functools.partial(layer_kernel, n_sp, n_tp, cap), out_shap...  83.7 us

profile of v1, /device:TPU:0, one launch (start us, length us, event | category | flops | bytes accessed | tf_op | source)
XLA Modules:
  0.0 85.4 jit_solution(3676099824632083675)
XLA Ops:
  0.0 83.7 %shard_map.172 = bf16[64,2048]{1,0:T(8,128)(2,1)} custom-call(bf16[256,256]{1,0:T(8,128)(2,1)} %d_hbm.1, f32[1,256]{1,0:T(1,128)} %bitcast.20, f32[4,256]{1,0:T(4,128)} %bitcast.17, bf16[256,256]{1,0:T(8,128)(2,1)} %k_hbm.1, bf16[256,512]{1,0:T(8,128)(2,1)} %v_hbm.1, bf16[256,256]{1,0:T(8,128)(2,1)} %q_hbm.1, bf16[256,512]{1,0:T(8,128)(2,1)} %g_hbm.1, ...), custom_call_target="tpu_custom_call" | custom-call | tf_op jit(solution)/shard_map/pallas_call | solution.py:705
  83.7 1.7 %copy.20 = bf16[64,2048]{1,0:T(8,128)(2,1)} copy(bf16[64,2048]{1,0:T(8,128)(2,1)} %shard_map.172) | data formatting | bytes 524288

commit v2 on v1

--- a/solution.py
+++ b/solution.py
@@ -73,17 +73,45 @@
     return high, mid, (rest - mid.astype(F32)).astype(BF16)
 
 
-def unit_order(n_sp):
-    half = n_sp // 2
-    pairs = [(i, 2) for i in range(0, half, 2)]
-    singles = [(i, 1) for i in range(half, n_sp)]
-    units = []
-    while pairs or singles:
-        if pairs:
-            units.append(pairs.pop(0))
-        if singles:
-            units.append(singles.pop(0))
-    return units
+def schedule(far, spare):
+    hooks = {}
+    start = 0
+    near = list(range(3, 3 + spare))
+    units = [1, 2] + list(range(3 + spare, 1 + spare + far))
+    end = 1 + spare + far
+
+    def put(k, slot, name, unit):
+        hooks.setdefault((k, slot), []).append((name, unit))
+
+    put(start, "first", "arr", units[1])
+    put(start, "up", "relay", units[0])
+    put(units[0], "up", "relay", units[1])
+    put(units[0], "down", "arr", units[2])
+    put(units[1], "first", "pass", units[0])
+    put(units[1], "up", "arr", units[3])
+    for k in near:
+        put(k - 1, "up", "relay", k)
+    put(near[0], "first", "pass", units[1])
+    put(near[0], "first", "pass", start)
+    put(near[-1], "up", "relay", units[2])
+    put(near[-1], "down", "give", units[0])
+    for t in range(2, far):
+        if t > 2:
+            put(units[t], "first", "give", units[t - 2])
+            put(units[t], "first", "pass", units[t - 1])
+        if t + 1 < far:
+            put(units[t], "up", "relay", units[t + 1])
+        if t + 2 < far:
+            put(units[t], "down", "arr", units[t + 2])
+    put(end, "first", "pass", units[-1])
+    for k in near:
+        put(end, "first", "pass", k)
+    put(end, "first", "give", units[-2])
+    put(end, "first", "give", start)
+    put(end, "first", "give", units[-1])
+    for k in near:
+        put(end, "first", "give", k)
+    return hooks
 
 
 def layer_kernel(
@@ -97,7 +125,7 @@
     ra, rb, tb, normed, xcol, sel_ref, mix_ref, outgoing, rows_ref, hidden, p_ref,
     r1, r2, ty, ob, back, acc, branch, brow, mid_ref,
     load, s_pair, r_pair, s_z, r_z,
-    sa, va, sb, vb, st, vt, ss, vs, sy, vy, sd, vd, s1, v1, s2, v2, s3, v3, s4, v4,
+    sa, va, vn, sb, vb, st, vt, ss, vs, sy, vy, sd, vd, s1, v1, s2, v2, s3, v3, s4, v4,
 ):
     me = lax.axis_index("sp")
     j = lax.axis_index("tp")
@@ -242,6 +270,34 @@
             )
             local.append(within + across)
 
+    def peer_of(i):
+        return flipped(me, i, n_sp)
+
+    with scope("a_route"):
+        loads[8].wait()
+        loads[9].wait()
+        e0, e1 = index_ref[0:1, :], index_ref[1:2, :]
+        named = lax.broadcasted_iota(jnp.int32, (n_sp, length), 0)
+        taken = jnp.where((named == e0) | (named == e1), 1.0, 0.0).astype(BF16)
+        before = jnp.where(row < col, 1.0, 0.0).astype(BF16)
+        counts = jnp.dot(taken, before, preferred_element_type=F32)
+
+        def target(e):
+            place = jnp.sum(jnp.where(named == e, counts, 0.0), axis=0, keepdims=True)
+            return e.astype(F32) * cap + place
+
+        t0, t1 = target(e0), target(e1)
+        w0, w1 = weight_ref[0:1, :], weight_ref[1:2, :]
+
+        def route(i):
+            slot = lax.broadcasted_iota(jnp.int32, (cap, length), 0) + peer_of(i) * cap
+            slot = slot.astype(F32)
+            is0, is1 = slot == t0, slot == t1
+            sel_ref[i] = jnp.where(is0 | is1, 1.0, 0.0).astype(BF16)
+            mix_ref[i] = (jnp.where(is0, w0, 0.0) + jnp.where(is1, w1, 0.0)).astype(BF16)
+
+        loop(n_sp, route)
+
     with scope("a_pair"):
         pair_copy.wait_recv()
         mine = message[side].astype(F32)
@@ -254,43 +310,15 @@
     def z_copy(i):
         return remote(
             zmsg, inbox.at[pair], s_z.at[i], r_z.at[pair],
-            {"sp": 2 * jnp.minimum(pair + 1 + i, n_pair - 1) + side},
+            {"sp": 2 * (n_pair - 1 - i) + side},
         )
 
     def z_send(i):
-        @pl.when(pair + 1 + i < n_pair)
+        @pl.when(n_pair - 1 - i > pair)
         def _():
             z_copy(i).start()
 
     loop(n_pair - 1, z_send)
-
-    def peer_of(i):
-        return flipped(me, i, n_sp)
-
-    with scope("a_route"):
-        loads[8].wait()
-        loads[9].wait()
-        e0, e1 = index_ref[0:1, :], index_ref[1:2, :]
-        named = lax.broadcasted_iota(jnp.int32, (n_sp, length), 0)
-        taken = jnp.where((named == e0) | (named == e1), 1.0, 0.0).astype(BF16)
-        before = jnp.where(row < col, 1.0, 0.0).astype(BF16)
-        counts = jnp.dot(taken, before, preferred_element_type=F32)
-
-        def target(e):
-            place = jnp.sum(jnp.where(named == e, counts, 0.0), axis=0, keepdims=True)
-            return e.astype(F32) * cap + place
-
-        t0, t1 = target(e0), target(e1)
-        w0, w1 = weight_ref[0:1, :], weight_ref[1:2, :]
-
-        def route(i):
-            slot = lax.broadcasted_iota(jnp.int32, (cap, length), 0) + peer_of(i) * cap
-            slot = slot.astype(F32)
-            is0, is1 = slot == t0, slot == t1
-            sel_ref[i] = jnp.where(is0 | is1, 1.0, 0.0).astype(BF16)
-            mix_ref[i] = (jnp.where(is0, w0, 0.0) + jnp.where(is1, w1, 0.0)).astype(BF16)
-
-        loop(n_sp, route)
 
     carried[...] = jnp.zeros_like(carried)
 
@@ -335,6 +363,12 @@
                 BF16
             )
 
+    def landed(ref, sem):
+        remote(ref, ref, sem, sem, {"sp": partner}).wait_recv()
+
+    def left(ref, sem):
+        remote(ref, ref, sem, sem, {"sp": partner}).wait_send()
+
     def rows_of(index):
         return pl.ds(pl.multiple_of(index * rows, rows), rows)
 
@@ -352,91 +386,109 @@
     def y_from(i):
         return lax.rem(y + n_y - 1 - i, n_y)
 
-    def head_pair(m, q):
+    cuts = 2 if rows % 32 == 0 else 1
+    band = rows // cuts
+
+    def band_of(index, r):
+        return pl.ds(pl.multiple_of(index * rows + r * band, band), band)
+
+    def head_pair(m, r, q):
         return remote(
-            part_ref.at[rows_of(2 * y_at(m) + 1 - c), piece_of(q)], ra.at[m, :, piece_of(q)],
-            sa.at[m, q], va.at[m, q], {"tp": sibling},
-        )
-
-    def head_far(m, q):
+            part_ref.at[band_of(2 * y_at(m) + 1 - c, r), piece_of(q)],
+            ra.at[m, band_of(0, r), piece_of(q)],
+            sa, va.at[m, r, q], {"tp": sibling},
+        )
+
+    def head_near(r):
         return remote(
-            tb.at[m, :, piece_of(q)], rb.at[m, :, piece_of(q)], sb.at[m, q], vb.at[m, q],
-            {"tp": 2 * y_at(m) + c},
-        )
-
-    def project(t):
-        m, q = t // PARTS, lax.rem(t, PARTS)
-        at = pl.ds(pl.multiple_of(2 * y_at(m) * rows, 2 * rows), 2 * rows)
-        part_ref[at, piece_of(q)] = jnp.dot(
-            gated[at, :], w_ref[:, piece_of(q)], preferred_element_type=F32
+            part_ref.at[band_of(sibling, r)], ra.at[n_y - 1, band_of(0, r)], sa, vn.at[r],
+            {"tp": sibling},
+        )
+
+    def head_far(m, r, q):
+        return remote(
+            tb.at[m, band_of(0, r), piece_of(q)], rb.at[m, band_of(0, r), piece_of(q)],
+            sb, vb.at[m, r, q], {"tp": 2 * y_at(m) + c},
+        )
+
+    def project(q):
+        part_ref[:, piece_of(q)] = jnp.dot(
+            gated[...], w_ref[:, piece_of(q)], preferred_element_type=F32
         ).astype(BF16)
-        head_pair(m, q).start()
-
-    def pair_sum(t):
-        m, q = t // PARTS, lax.rem(t, PARTS)
-        head_pair(m, q).wait_recv()
-        tb[m, :, piece_of(q)] = (
-            part_ref[rows_of(2 * y_at(m) + c), piece_of(q)].astype(F32)
-            + ra[m, :, piece_of(q)].astype(F32)
+        for m in range(n_y - 1):
+            for r in range(cuts):
+                head_pair(m, r, q).start()
+
+    def pair_sum(m, r, q):
+        head_pair(m, r, q).wait_recv()
+        at, cols = band_of(0, r), piece_of(q)
+        tb[m, at, cols] = (
+            part_ref[band_of(2 * y_at(m) + c, r), cols].astype(F32) + ra[m, at, cols].astype(F32)
         ).astype(BF16)
-        head_far(m, q).start()
-
-    def whole_sum(q):
-        head_pair(n_y - 1, q).wait_recv()
-        total = part_ref[rows_of(j), piece_of(q)].astype(F32) + ra[
-            n_y - 1, :, piece_of(q)
-        ].astype(F32)
+        head_far(m, r, q).start()
+
+    def whole_sum(r, q):
+        at, cols = band_of(0, r), piece_of(q)
+        total = part_ref[band_of(j, r), cols].astype(F32) + ra[n_y - 1, at, cols].astype(F32)
         for m in range(n_y - 1):
-            head_far(m, q).wait_recv()
-            total = total + rb[m, :, piece_of(q)].astype(F32)
-        mixed_ref[:, piece_of(q)] = total
+            head_far(m, r, q).wait_recv()
+            total = total + rb[m, at, cols].astype(F32)
+        mixed_ref[at, cols] = total
+
+    def turn_copy(r, i):
+        peer = lax.rem(j + 1 + i, n_tp)
+        return remote(
+            normed.at[band_of(0, r), cols_of(peer)], xcol.at[band_of(j, r)],
+            st, vt, {"tp": peer},
+        )
 
     with scope("e_proj"):
         loads[10].wait()
-        loop(n_y * PARTS, project)
+        loop(PARTS, project)
+        for r in range(cuts):
+            head_near(r).start()
     with scope("e_pair"):
-        loop((n_y - 1) * PARTS, pair_sum)
-    with scope("e_rs"):
-        loop(PARTS, whole_sum)
-    with scope("e_norm"):
+        for r in range(cuts):
+            loop((n_y - 1) * PARTS, lambda t: pair_sum(t // PARTS, r, lax.rem(t, PARTS)))
         for copy in loads[11:15]:
             copy.wait()
-        mid = (res_ref[...].astype(F32) + rms_scale(mixed_ref[...], again_ref[...])).astype(BF16)
-        mid_ref[...] = mid
-        normed[...] = rms_scale(mid.astype(F32), bgain_ref[...]).astype(BF16)
-
-    def turn_copy(i):
-        peer = lax.rem(j + 1 + i, n_tp)
-        return remote(
-            normed.at[:, cols_of(peer)], xcol.at[rows_of(j)], st.at[i], vt.at[i], {"tp": peer}
-        )
-
+    for r in range(cuts):
+        at = slice(r * band, (r + 1) * band)
+        with scope(f"e_rs{r}"):
+            head_near(r).wait_recv()
+            loop(PARTS, lambda q: whole_sum(r, q))
+        with scope(f"e_norm{r}"):
+            mid = (
+                res_ref[at, :].astype(F32) + rms_scale(mixed_ref[at, :], again_ref[...])
+            ).astype(BF16)
+            mid_ref[at, :] = mid
+            normed[at, :] = rms_scale(mid.astype(F32), bgain_ref[...]).astype(BF16)
+        loop(n_tp - 1, lambda i: turn_copy(r, i).start())
+        xcol[band_of(j, r), :] = normed[at, cols_of(j)]
     with scope("e_turn"):
-        loop(n_tp - 1, lambda i: turn_copy(i).start())
-        xcol[rows_of(j), :] = normed[:, cols_of(j)]
-        loop(n_tp - 1, lambda i: turn_copy(i).wait_recv())
+        landed(xcol.at[0 : (n_tp - 1) * rows], vt)
 
     def picked(i):
         return jnp.dot(sel_ref[i], xcol[...], preferred_element_type=F32).astype(BF16)
 
     def out_copy(i):
         return remote(
-            outgoing.at[i], rows_ref.at[i, :, cols_of(j)], ss.at[i], vs.at[i],
+            outgoing.at[i], rows_ref.at[i, :, cols_of(j)], ss, vs.at[i],
             {"sp": peer_of(i)},
         )
 
     def y_copy(i, m):
         place = rows_ref.at[i, :, cols_of(j)]
-        return remote(place, place, sy.at[m, i], vy.at[m, i], {"tp": 2 * y_at(m) + c})
-
-    def pair_forward(i, m, owner):
+        return remote(place, place, sy, vy.at[m, i], {"tp": 2 * y_at(m) + c})
+
+    def pair_forward(i, owner):
         place = rows_ref.at[i, :, cols_of(owner)]
-        return remote(place, place, sd.at[m, i], vd.at[m, i], {"tp": sibling})
+        return remote(place, place, sd, vd.at[i], {"tp": sibling})
 
     def forward(i):
         for m in range(n_y - 1):
             y_copy(i, m).start()
-        pair_forward(i, n_y - 1, j).start()
+        pair_forward(i, j).start()
 
     def arrived(i):
         out_copy(i).wait_recv()
@@ -445,26 +497,25 @@
     def relay(i):
         for m in range(n_y - 1):
             y_copy(i, m).wait_recv()
-            pair_forward(i, m, 2 * y_from(m) + c).start()
+            pair_forward(i, 2 * y_from(m) + c).start()
 
     def ready(i):
-        for m in range(n_y - 1):
-            pair_forward(i, m, 2 * y_from(m) + c).wait_recv()
-        pair_forward(i, n_y - 1, j).wait_recv()
+        landed(rows_ref.at[i, :, 0 : n_y * share], vd.at[i])
 
     def part_pair(i, m):
         return remote(
             p_ref.at[i, :, cols_of(2 * y_at(m) + 1 - c)], r1.at[i, m],
-            s1.at[i, m], v1.at[i, m], {"tp": sibling},
+            s1, v1.at[i, m], {"tp": sibling},
         )
 
     def part_far(i, m):
         return remote(
-            ty.at[i, m], r2.at[i, m], s2.at[i, m], v2.at[i, m], {"tp": 2 * y_at(m) + c}
-        )
-
-    def back_copy(i):
-        return remote(ob.at[i], back.at[i], s3.at[i], v3.at[i], {"sp": peer_of(i)})
+            ty.at[i, m], r2.at[i, m], s2, v2.at[i, m], {"tp": 2 * y_at(m) + c}
+        )
+
+    def back_copy(i, h):
+        slot = i if h == 0 else jnp.where(i == n_sp - 1, n_sp, i)
+        return remote(ob.at[h, i], back.at[h, i], s3, v3.at[slot], {"sp": peer_of(i)})
 
     def pass_along(i):
         for m in range(n_y - 1):
@@ -483,164 +534,167 @@
         return total.astype(BF16)
 
     def give_back(i):
-        if i == 0:
-            back[0] = summed(0)
-        else:
-            ob[i] = summed(i)
-            back_copy(i).start()
-
+        total = summed(i)
+        for h in range(2):
+            if isinstance(i, int) and i == 0:
+                back[h, 0] = total[:, h * narrow : (h + 1) * narrow]
+            else:
+                ob[h, i] = total[:, h * narrow : (h + 1) * narrow]
+                back_copy(i, h).start()
+
+    narrow = share // 2
     tile = min(TILE, wg.shape[1])
     steps = wg.shape[1] // tile
 
-    def run_expert(first, count, after_first_up, after_up, after_first_down):
+    def run_expert(first, count, after_first, after_up, after_first_down):
         batch = count * cap
 
-        def up(t):
-            cols = pl.ds(pl.multiple_of(t * tile, tile), tile)
-            fed = rows_ref[first : first + count].reshape(batch, model)
+        for t in range(steps):
+            cols = slice(t * tile, (t + 1) * tile)
+            fed = rows_ref[pl.ds(first, count)].reshape(batch, model)
             gate = jnp.dot(fed, wg[:, cols], preferred_element_type=F32)
             rise = jnp.dot(fed, wu[:, cols], preferred_element_type=F32)
             hidden[0:batch, cols] = (gate * jax.nn.sigmoid(gate) * rise).astype(BF16)
 
-            @pl.when(t == 0)
-            def _():
-                after_first_up()
-
-        loop(steps, up)
+            if t == 0:
+                after_first()
         after_up()
 
-        def down(owner):
-            made = jnp.dot(hidden[0:batch, :], wd[:, cols_of(owner)], preferred_element_type=F32)
-            p_ref[first : first + count, :, cols_of(owner)] = made.astype(BF16).reshape(
-                count, cap, share
+        def down(m):
+            cols = pl.ds(pl.multiple_of(2 * y_at(m) * share, 2 * share), 2 * share)
+            made = jnp.dot(hidden[0:batch, :], wd[:, cols], preferred_element_type=F32)
+            p_ref[pl.ds(first, count), :, cols] = made.astype(BF16).reshape(
+                count, cap, 2 * share
             )
-
-        def down_pair(m):
-            down(2 * y_at(m) + 1 - c)
             for i in range(count):
                 part_pair(first + i, m).start()
-            down(2 * y_at(m) + c)
 
             @pl.when(m == 0)
             def _():
                 after_first_down()
 
-        loop(n_y, down_pair)
-
-    units = unit_order(n_sp)
+        loop(n_y, down)
+
+    inner = (4 * pair >= n_pair) & (4 * pair < 3 * n_pair)
+    spare = [(i, 2) for i in range(2, half, 2)]
+    units = (
+        [(0, 2), (half, 1), (half + 1, 1)] + spare + [(i, 1) for i in range(half + 2, n_sp)]
+    )
     total_units = len(units)
-
-    def each(k, body):
-        if 0 <= k < total_units:
-            for i in range(units[k][0], units[k][0] + units[k][1]):
-                body(i)
-
-    def arrive(k):
-        each(k, lambda i: arrived(i) if i > 0 else None)
+    acts = {"arr": arrived, "relay": relay, "ready": ready, "pass": pass_along, "give": give_back}
+    hooks = schedule(half, len(spare))
+
+    def act(name, k):
+        first, count = units[k]
+        for i in range(count):
+            if name == "arr" and k == 0 and i == 0:
+                continue
+            with scope(f"w_{name}{k}{i}"):
+                acts[name](first + i)
+
+    def fire(k, slot):
+        for name, other in hooks.get((k, slot), ()):
+            act(name, other)
 
     with scope("e_send"):
         rows_ref[0, :, cols_of(j)] = picked(0)
         forward(0)
 
         def send(t):
-            i = jnp.where(lax.rem(t, 2) == 0, half + t // 2, 1 + t // 2)
+            lead = half // 2
+            far_first = jnp.where(
+                t < lead, half + t, jnp.where(t < lead + half - 1, t - lead + 1, t + 1)
+            )
+            i = jnp.where(inner, t + 1, far_first)
             outgoing[i] = picked(i)
             out_copy(i).start()
 
         loop(n_sp - 1, send)
     with scope("e_arrive"):
-        arrive(0)
+        act("arr", 0)
         relay(0)
-        arrive(1)
-        arrive(2)
+        arrived(2)
+        act("arr", 1)
     with scope("e_relay"):
-        for i in range(1, units[0][1]):
-            relay(i)
+        relay(1)
+        for i in range(3, half):
+            with scope(f"w_near{i}"):
+                arrived(i)
     with scope("e_weights"):
         for copy in loads[15:]:
             copy.wait()
     for k, (first, count) in enumerate(units):
         with scope(f"e_ready{k}"):
-            each(k, ready)
+            act("ready", k)
         with scope(f"e_run{k}"):
             run_expert(
-                first,
-                count,
-                lambda: each(k - 1, pass_along),
-                lambda: each(k + 1, relay),
-                lambda: each(k - 2, give_back),
+                first, count, lambda: fire(k, "first"), lambda: fire(k, "up"),
+                lambda: fire(k, "down"),
             )
-        with scope(f"e_arrive{k}"):
-            arrive(k + 3)
     with scope("e_give"):
-        each(total_units - 1, pass_along)
-        each(total_units - 2, give_back)
-        each(total_units - 1, give_back)
-
-    def weighed(i):
-        return contract(mix_ref[i], back[i], 0, 0)
-
-    with scope("e_gather"):
-        acc[...] = weighed(0)
-
-        def gather(t):
-            back_copy(t + 1).wait_recv()
-            acc[...] = acc[...] + weighed(t + 1)
-
-        loop(n_sp - 2, gather)
-        back_copy(n_sp - 1).wait_recv()
-        branch[...] = (acc[...] + weighed(n_sp - 1)).astype(BF16)
-
-    def home_copy(i):
+        fire(total_units, "first")
+
+    def weighed(i, h):
+        return contract(mix_ref[i], back[h, i], 0, 0)
+
+    def home_copy(h, i):
         peer = lax.rem(j + 1 + i, n_tp)
         return remote(
-            branch.at[rows_of(peer)], brow.at[:, cols_of(j)], s4.at[i], v4.at[i], {"tp": peer}
-        )
-
-    with scope("e_home"):
-        loop(n_tp - 1, lambda i: home_copy(i).start())
-        brow[:, cols_of(j)] = branch[rows_of(j), :]
-        loop(n_tp - 1, lambda i: home_copy(i).wait_recv())
-    with scope("e_out"):
-        out_ref[...] = (
-            mid_ref[...].astype(F32) + rms_scale(brow[...].astype(F32), fgain_ref[...])
-        ).astype(BF16)
+            branch.at[h, rows_of(peer)], brow.at[j, h], s4, v4, {"tp": peer}
+        )
+
+    with scope("e_gather"):
+        for h in range(2):
+            acc[h] = weighed(0, h)
+
+        def gather(i):
+            with scope("w_back"):
+                landed(back.at[:, i], v3.at[i])
+            for h in range(2):
+                acc[h] = acc[h] + weighed(i, h)
+
+        loop(half - 1, lambda t: gather(half + t))
+        loop(half - 1, lambda t: gather(1 + t))
+        for h in range(2):
+            back_copy(n_sp - 1, h).wait_recv()
+            branch[h] = (acc[h] + weighed(n_sp - 1, h)).astype(BF16)
+            loop(n_tp - 1, lambda i: home_copy(h, i).start())
+            brow[j, h] = branch[h, rows_of(j), :]
 
     with scope("e_drain"):
         pair_copy.wait_send()
         exch_copy.wait_send()
 
         def drain_z(i):
-            @pl.when(pair + 1 + i < n_pair)
+            @pl.when(n_pair - 1 - i > pair)
             def _():
                 z_copy(i).wait_send()
 
         loop(n_pair - 1, drain_z)
-        loop(n_y * PARTS, lambda t: head_pair(t // PARTS, lax.rem(t, PARTS)).wait_send())
-        loop((n_y - 1) * PARTS, lambda t: head_far(t // PARTS, lax.rem(t, PARTS)).wait_send())
-
-        def drain_sp(i):
-            out_copy(i + 1).wait_send()
-            back_copy(i + 1).wait_send()
-
-        loop(n_sp - 1, drain_sp)
-
-        def drain_turns(i):
-            turn_copy(i).wait_send()
-            home_copy(i).wait_send()
-
-        loop(n_tp - 1, drain_turns)
-
-        def drain(i):
-            for m in range(n_y - 1):
-                y_copy(i, m).wait_send()
-                pair_forward(i, m, 2 * y_from(m) + c).wait_send()
-                part_far(i, m).wait_send()
-            pair_forward(i, n_y - 1, j).wait_send()
-            for m in range(n_y):
-                part_pair(i, m).wait_send()
-
-        loop(n_sp, drain)
+        left(part_ref.at[0 : n_y * rows], sa)
+        left(tb.at[0 : n_y - 1], sb)
+        left(normed.at[:, 0 : (n_tp - 1) * share], st)
+        left(outgoing.at[1:n_sp], ss)
+        left(rows_ref.at[:, :, 0 : (n_y - 1) * share], sy)
+        left(rows_ref.at[:, :, 0 : n_y * share], sd)
+        left(p_ref.at[:, :, 0 : n_y * share], s1)
+        left(p_ref.at[:, :, 0 : (n_y - 1) * share], s2)
+        left(ob.at[:, 1:n_sp], s3)
+    with scope("e_home"):
+        landed(brow.at[0 : n_tp - 1], v4)
+    with scope("e_out"):
+        places = [(s, h) for s in range(n_tp) for h in range(2)]
+        square = sum(
+            jnp.sum(brow[s, h].astype(F32) * brow[s, h].astype(F32), axis=-1, keepdims=True)
+            for s, h in places
+        )
+        scale = lax.rsqrt(square * (1.0 / model) + EPSILON)
+        for s, h in places:
+            cols = slice(s * share + h * narrow, s * share + (h + 1) * narrow)
+            out_ref[:, cols] = (
+                mid_ref[:, cols].astype(F32) + brow[s, h].astype(F32) * scale * fgain_ref[:, cols]
+            ).astype(BF16)
+        left(branch.at[:, 0 : (n_tp - 1) * rows], s4)
 
 
 def dmas(*shapes):
@@ -733,19 +787,18 @@
             pltpu.VMEM(by_peer + (cap, share), BF16),
             pltpu.VMEM(by_peer + (cap, share), BF16),
             pltpu.VMEM(by_peer + (cap, share), BF16),
-            pltpu.VMEM((n_sp, cap, share), BF16),
-            pltpu.VMEM((n_sp, cap, share), BF16),
-            pltpu.VMEM((length, share), F32),
-            pltpu.VMEM((length, share), BF16),
-            pltpu.VMEM((rows, model), BF16),
+            pltpu.VMEM((2, n_sp, cap, share // 2), BF16),
+            pltpu.VMEM((2, n_sp, cap, share // 2), BF16),
+            pltpu.VMEM((2, length, share // 2), F32),
+            pltpu.VMEM((2, length, share // 2), BF16),
+            pltpu.VMEM((n_tp, 2, rows, share // 2), BF16),
             pltpu.VMEM((rows, model), BF16),
         ]
         + dmas(
             (len(operands),), (2,), (2,), (n_sp // 2,), (n_sp // 2,),
-            (n_y, PARTS), (n_y, PARTS), (n_y, PARTS), (n_y, PARTS),
-            (n_tp,), (n_tp,), (n_sp,), (n_sp,),
-            (n_y, n_sp), (n_y, n_sp), (n_y, n_sp), (n_y, n_sp),
-            by_peer, by_peer, by_peer, by_peer, (n_sp,), (n_sp,), (n_tp,), (n_tp,),
+            (), (n_y - 1, 2, PARTS), (2,), (), (n_y - 1, 2, PARTS), (), (), (), (n_sp,),
+            (), (n_y - 1, n_sp), (), (n_sp,), (), by_peer, (), by_peer,
+            (), (n_sp + 1,), (), (),
         ),
         compiler_params=pltpu.CompilerParams(
             collective_id=1, has_side_effects=True, vmem_limit_bytes=VMEM_LIMIT

time: 86.6 us -> 80 us (0.924)
  Pallas kernels: 83.7 us -> 77.9 us
    pallas_call x1, Pallas kernels: 83.7 us -> 77.9 us  [shards(): pl.pallas_call(functools.partial(layer_kernel, n_sp, n_tp, cap), out_shap...]
where the time goes in v2:
time: 80 us; the launch traced here: 79.6 us
  Pallas kernels  77.9 us (97%)
  local copies, waits for them, and re-layouts  1.67 us (2%)
    pallas_call x1, Pallas kernels, shards(): pl.pallas_call(functools.partial(layer_kernel, n_sp, n_tp, cap), out_shap...  77.9 us
    unnamed x1, local copies, waits for them, and re-layouts  1.67 us

profile of v2, /device:TPU:0, one launch (start us, length us, event | category | flops | bytes accessed | tf_op | source)
XLA Modules:
  0.0 79.6 jit_solution(10972661564075255230)
XLA Ops:
  0.0 77.9 %shard_map.172 = bf16[64,2048]{1,0:T(8,128)(2,1)} custom-call(bf16[256,256]{1,0:T(8,128)(2,1)} %d_hbm.1, f32[1,256]{1,0:T(1,128)} %bitcast.20, f32[4,256]{1,0:T(4,128)} %bitcast.17, bf16[256,256]{1,0:T(8,128)(2,1)} %k_hbm.1, bf16[256,512]{1,0:T(8,128)(2,1)} %v_hbm.1, bf16[256,256]{1,0:T(8,128)(2,1)} %q_hbm.1, bf16[256,512]{1,0:T(8,128)(2,1)} %g_hbm.1, ...), custom_call_target="tpu_custom_call" | custom-call | tf_op jit(solution)/shard_map/pallas_call | solution.py:759
  77.9 1.7 %copy.20 = bf16[64,2048]{1,0:T(8,128)(2,1)} copy(bf16[64,2048]{1,0:T(8,128)(2,1)} %shard_map.172) | data formatting | bytes 524288

commit v3 on v2

--- a/solution.py
+++ b/solution.py
@@ -21,7 +21,7 @@
 BF16 = jnp.bfloat16
 FADE_ROWS = 16
 PARTS = 4
-TILE = 512
+TILE = 1024
 VMEM_LIMIT = 67043328
 
 
@@ -83,8 +83,9 @@
     def put(k, slot, name, unit):
         hooks.setdefault((k, slot), []).append((name, unit))
 
-    put(start, "first", "arr", units[1])
     put(start, "up", "relay", units[0])
+    for k in near[1:]:
+        put(start, "down", "arr", k)
     put(units[0], "up", "relay", units[1])
     put(units[0], "down", "arr", units[2])
     put(units[1], "first", "pass", units[0])
@@ -256,7 +257,9 @@
         local = []
         for h in range(heads):
             cs = slice(h * KEY_CHANNELS, (h + 1) * KEY_CHANNELS)
-            scores = jnp.where(causal, contract(q_in[:, cs], k_inv[:, cs], 1, 1), 0.0).astype(BF16)
+            own = jnp.sum(q[:, cs] * k[:, cs], axis=1, keepdims=True)
+            scores = jnp.where(causal, contract(q_in[:, cs], k_inv[:, cs], 1, 1), 0.0)
+            scores = jnp.where(row == col, own, scores).astype(BF16)
             within = jnp.dot(scores, v_ref[:, h * DV : (h + 1) * DV], preferred_element_type=F32)
             across = jnp.concatenate(
                 [jnp.zeros((BLOCK, DV), F32)]
@@ -543,11 +546,10 @@
                 back_copy(i, h).start()
 
     narrow = share // 2
-    tile = min(TILE, wg.shape[1])
-    steps = wg.shape[1] // tile
-
-    def run_expert(first, count, after_first, after_up, after_first_down):
+    def run_expert(first, count, last, after_first, after_up, after_first_down):
         batch = count * cap
+        tile = min(TILE // 2 if last else TILE, wg.shape[1])
+        steps = wg.shape[1] // tile
 
         for t in range(steps):
             cols = slice(t * tile, (t + 1) * tile)
@@ -592,7 +594,19 @@
             with scope(f"w_{name}{k}{i}"):
                 acts[name](first + i)
 
+    def second_poll():
+        with scope("w_poll2"):
+            arrived(jnp.where(top, 2, half + 1))
+
+    def third_poll():
+        with scope("w_poll3"):
+            arrived(3)
+
     def fire(k, slot):
+        if k == 0 and slot == "first":
+            second_poll()
+        if k == 0 and slot == "down":
+            third_poll()
         for name, other in hooks.get((k, slot), ()):
             act(name, other)
 
@@ -613,13 +627,11 @@
     with scope("e_arrive"):
         act("arr", 0)
         relay(0)
-        arrived(2)
         act("arr", 1)
     with scope("e_relay"):
         relay(1)
-        for i in range(3, half):
-            with scope(f"w_near{i}"):
-                arrived(i)
+        top = pair == n_pair - 1
+        arrived(jnp.where(top, half + 1, 2))
     with scope("e_weights"):
         for copy in loads[15:]:
             copy.wait()
@@ -628,8 +640,8 @@
             act("ready", k)
         with scope(f"e_run{k}"):
             run_expert(
-                first, count, lambda: fire(k, "first"), lambda: fire(k, "up"),
-                lambda: fire(k, "down"),
+                first, count, k == total_units - 1, lambda: fire(k, "first"),
+                lambda: fire(k, "up"), lambda: fire(k, "down"),
             )
     with scope("e_give"):
         fire(total_units, "first")

time: 80 us -> 79 us (0.988)
  no operation moved by 1% of the time
where the time goes in v3:
time: 79 us; the launch traced here: 78.9 us
  Pallas kernels  77.2 us (98%)
  local copies, waits for them, and re-layouts  1.67 us (2%)
    pallas_call x1, Pallas kernels, shards(): pl.pallas_call(functools.partial(layer_kernel, n_sp, n_tp, cap), out_shap...  77.2 us
    unnamed x1, local copies, waits for them, and re-layouts  1.67 us

profile of v3, /device:TPU:0, one launch (start us, length us, event | category | flops | bytes accessed | tf_op | source)
XLA Modules:
  0.0 78.9 jit_solution(241603764292495954)
XLA Ops:
  0.0 77.2 %shard_map.172 = bf16[64,2048]{1,0:T(8,128)(2,1)} custom-call(bf16[256,256]{1,0:T(8,128)(2,1)} %d_hbm.1, f32[1,256]{1,0:T(1,128)} %bitcast.20, f32[4,256]{1,0:T(4,128)} %bitcast.17, bf16[256,256]{1,0:T(8,128)(2,1)} %k_hbm.1, bf16[256,512]{1,0:T(8,128)(2,1)} %v_hbm.1, bf16[256,256]{1,0:T(8,128)(2,1)} %q_hbm.1, bf16[256,512]{1,0:T(8,128)(2,1)} %g_hbm.1, ...), custom_call_target="tpu_custom_call" | custom-call | tf_op jit(solution)/shard_map/pallas_call | solution.py:771
  77.2 1.7 %copy.20 = bf16[64,2048]{1,0:T(8,128)(2,1)} copy(bf16[64,2048]{1,0:T(8,128)(2,1)} %shard_map.172) | data formatting | bytes 524288
